TPU v7x, 32 devices: a whole 2x2x4 slice. The times are simulated.
32 devices in a mesh: sp: 16 (over z, y, x), tp: 2 (over core).
Axes of the slice: x: 2, y: 2, z: 4, core: 2. Of those that a mesh axis runs over, the one named last changes fastest.
Arguments:
- stream: bfloat16 [4096, 2048], P(('sp', 'tp')), may hold values from -6 to 6
- head_input_signal: bfloat16 [4096, 2048], P('sp', 'tp'), may hold values from -6 to 6
- write_input_vectors: bfloat16 [4096, 512], P('sp', 'tp'), may hold values from -6 to 6
- read_input_vectors: bfloat16 [4096, 512], P('sp', 'tp'), may hold values from -6 to 6
- output_gate_input: bfloat16 [4096, 2048], P('sp', 'tp'), may hold values from -6 to 6
- step_size_input: bfloat16 [4096, 32], P('sp', 'tp'), may hold values from -5 to 5.5
- position_log_decay: float32 [4096, 32], P('sp', 'tp'), may hold values from -0.7 to 0
- signal_filter_taps: bfloat16 [4, 2048], P(None, 'tp'), may hold values from -3 to 3
- write_filter_taps: bfloat16 [4, 512], P(None, 'tp'), may hold values from -3 to 3
- read_filter_taps: bfloat16 [4, 512], P(None, 'tp'), may hold values from -3 to 3
- step_size_bias: float32 [32], P('tp'), may hold values from -1 to 1
- head_decay_rate: float32 [32], P('tp'), may hold values from 2.4414063e-06 to 0.03
- head_direct_term: float32 [32], P('tp'), may hold values from 0.5 to 2
- grouped_norm_gain: float32 [2048], P('tp'), may hold values from 0.1 to 1.9
- mixer_output_weight: bfloat16 [2048, 2048], P('tp'), may hold values from -0.125 to 0.125
- expert_norm_gain: float32 [2048], replicated, may hold values from 0.1 to 1.9
- chosen_expert_index: int32 [4096, 4], P(('sp', 'tp')), may hold values from 0 to 31, all different within a row; in each aligned block of 128 rows (0 to 127, 128 to 255, ...) at most 24 rows name the same one
- chosen_expert_weight: float32 [4096, 4], P(('sp', 'tp')), may hold values from 0.1 to 1
- routed_gate_weight: bfloat16 [32, 2048, 512], P(('sp', 'tp')), may hold values from -0.125 to 0.125
- routed_up_weight: bfloat16 [32, 2048, 512], P(('sp', 'tp')), may hold values from -0.125 to 0.125
- routed_down_weight: bfloat16 [32, 512, 2048], P(('sp', 'tp')), may hold values from -0.25 to 0.25
- common_gate_weight: bfloat16 [2048, 512], replicated, may hold values from -0.125 to 0.125
- common_up_weight: bfloat16 [2048, 512], replicated, may hold values from -0.125 to 0.125
- common_down_weight: bfloat16 [512, 2048], replicated, may hold values from -0.25 to 0.25
Outputs:
- layer_out: bfloat16 [4096, 2048], P(('sp', 'tp'))
Inputs may be any that keep to these rules, and one draw needn't show every extreme that they name: `chosen_expert_index`: each row names 4 different experts. Among the 128 rows of one device (aligned blocks of 128 rows) no expert is named more than 24 times; in some block one expert is named exactly 24 times.
All inputs are finite; a program needn't handle non-finite values.
Results may differ from a plain program's by a relative error of at most 0.015.
Values may be sent and summed in bfloat16 or wider, within the bound.
A program may use at most 128 MiB of HBM per device.

v0:
```python
import jax
import jax.numpy as jnp
from jax import lax
from jax.sharding import PartitionSpec as P

HEAD_DIM = 64
STATE = 128
BLK = 128


precise = lax.Precision.HIGHEST


def from_behind(block, axis, distance):
    devices = range(lax.axis_size(axis))
    route = [(i - distance, i) for i in devices if i - distance in devices]
    return lax.ppermute(block, axis, route)


def carried_in(value, axis, join, neutral):
    count, mine = (lax.axis_size(axis), lax.axis_index(axis))
    pieces = jax.tree.map(lambda part: lax.all_gather(part, axis), value)
    subtotal = jax.tree.map(
        lambda part, zero: jnp.full_like(part, 0) + jnp.asarray(zero, part.dtype), value, neutral
    )

    def lap(position, subtotal):
        longer = join(subtotal, jax.tree.map(lambda part: part[position], pieces))
        return jax.tree.map(lambda new, old: jnp.where(position < mine, new, old), longer, subtotal)

    return lax.fori_loop(0, count - 1, lap, subtotal)


def causal_conv(previous, current, weight):
    stacked = jnp.concatenate([previous, current], axis=0).astype(jnp.float32)
    weight = weight.astype(jnp.float32)
    kernel_len = weight.shape[0]
    length = current.shape[0]
    summed_taps = weight[0] * stacked[0:length]
    for offset in range(1, kernel_len):
        summed_taps = summed_taps + weight[offset] * stacked[offset : offset + length]
    return jax.nn.silu(summed_taps)


def combine(earlier, latter):
    return (earlier[0] * latter[0], earlier[1] * latter[0][..., None, None] + latter[1])


def advance(carry_state, inputs):
    block_piece, decay_factor = inputs
    return (carry_state * decay_factor[..., None, None] + block_piece, carry_state)


def on_device(
    stream,
    head_input_signal,
    write_input_vectors,
    read_input_vectors,
    output_gate_input,
    step_size_input,
    position_log_decay,
    signal_filter_taps,
    write_filter_taps,
    read_filter_taps,
    step_size_bias,
    head_decay_rate,
    head_direct_term,
    grouped_norm_gain,
    mixer_output_weight,
    expert_norm_gain,
    chosen_expert_index,
    chosen_expert_weight,
    routed_gate_weight,
    routed_up_weight,
    routed_down_weight,
    common_gate_weight,
    common_up_weight,
    common_down_weight,
):
    length = head_input_signal.shape[0]
    margin = signal_filter_taps.shape[0] - 1
    head_count = step_size_input.shape[1]
    groups = write_input_vectors.shape[1] // STATE
    per_group = head_count // groups
    blocks = length // BLK
    rim_rows = (
        head_input_signal[length - margin :],
        write_input_vectors[length - margin :],
        read_input_vectors[length - margin :],
    )
    before = from_behind((rim_rows[0], rim_rows[1], rim_rows[2]), "sp", 1)
    signal = causal_conv(before[0], head_input_signal, signal_filter_taps)
    write_vec = causal_conv(before[1], write_input_vectors, write_filter_taps)
    read_vec = causal_conv(before[2], read_input_vectors, read_filter_taps)
    time_position = jax.nn.softplus(step_size_input.astype(jnp.float32) + step_size_bias)
    decay_logarithm = position_log_decay - head_decay_rate * time_position
    signal_heads = signal.reshape(blocks, BLK, groups, per_group, HEAD_DIM)
    scaled_blocks = signal_heads * time_position.reshape(blocks, BLK, groups, per_group)[..., None]
    write_blocks = write_vec.reshape(blocks, BLK, groups, STATE)
    read_blocks = read_vec.reshape(blocks, BLK, groups, STATE)
    within_cum = jnp.cumsum(decay_logarithm.reshape(blocks, BLK, groups, per_group), axis=1)
    block_total = within_cum[:, -1]
    running = jnp.cumsum(block_total, axis=0)
    device_total = running[-1]
    causal = jnp.arange(BLK)[:, None] >= jnp.arange(BLK)[None, :]
    cum_heads = jnp.transpose(within_cum, (0, 2, 3, 1))
    differences = cum_heads[..., :, None] - cum_heads[..., None, :]
    decay_matrix = jnp.exp(jnp.where(causal, differences, -jnp.inf))
    intersection = jnp.einsum("btgn,bsgn->bgts", read_blocks, write_blocks, precision=precise)
    intra_out = jnp.einsum(
        "bgts,bgets,bsgep->btgep", intersection, decay_matrix, scaled_blocks, precision=precise
    )
    tail_decay = jnp.exp(block_total[:, None] - within_cum)
    block_states = jnp.einsum(
        "bsgn,bsge,bsgep->bgepn", write_blocks, tail_decay, scaled_blocks, precision=precise
    )
    device_state = jnp.einsum(
        "bgepn,bge->gepn", block_states, jnp.exp(device_total[None] - running), precision=precise
    )
    identity = (jnp.ones_like(device_total), jnp.zeros_like(device_state))
    incoming = carried_in((jnp.exp(device_total), device_state), "sp", combine, identity)[1]
    readout_scale = jnp.exp(within_cum)
    start_states = lax.scan(advance, incoming, (block_states, jnp.exp(block_total)))[1]
    near_out = jnp.einsum(
        "btgn,bgepn,btge->btgep", read_blocks, start_states, readout_scale, precision=precise
    )
    ssd_out = intra_out + near_out
    ssd_out = ssd_out + head_direct_term.reshape(groups, per_group)[:, :, None] * signal_heads
    gated = ssd_out.reshape(length, groups, per_group * HEAD_DIM) * jax.nn.silu(
        output_gate_input.astype(jnp.float32)
    ).reshape(length, groups, per_group * HEAD_DIM)
    norm_scale = lax.rsqrt(jnp.mean(gated * gated, axis=-1, keepdims=True) + 1e-06)
    mixer_out = ((gated * norm_scale).reshape(length, -1) * grouped_norm_gain).astype(jnp.bfloat16)
    row_count = stream.shape[0]
    summed = lax.psum_scatter(
        jnp.dot(mixer_out, mixer_output_weight, preferred_element_type=jnp.float32).astype(
            jnp.bfloat16
        ),
        "tp",
        scatter_dimension=0,
        tiled=True,
    ).astype(jnp.float32)
    residual = (stream.astype(jnp.float32) + summed).astype(jnp.bfloat16)
    widened = residual.astype(jnp.float32)
    normed = (
        widened
        * lax.rsqrt(jnp.mean(widened * widened, axis=-1, keepdims=True) + 1e-06)
        * expert_norm_gain
    ).astype(jnp.bfloat16)
    shared_hidden = (
        jax.nn.silu(jnp.dot(normed, common_gate_weight, preferred_element_type=jnp.float32))
        * jnp.dot(normed, common_up_weight, preferred_element_type=jnp.float32)
    ).astype(jnp.bfloat16)
    shared = jnp.dot(shared_hidden, common_down_weight, preferred_element_type=jnp.float32)
    sp_count = lax.axis_size("sp")
    tp_count = lax.axis_size("tp")
    experts = sp_count * tp_count
    fanout = chosen_expert_index.shape[1]
    capacity = max(2, (3 * row_count * fanout + 2 * experts - 1) // (2 * experts))
    chosen = chosen_expert_index.reshape(-1)
    one_hot = (chosen[:, None] == jnp.arange(experts, dtype=jnp.int32)[None, :]).astype(jnp.int32)
    slot_index = jnp.sum((jnp.cumsum(one_hot, axis=0) - one_hot) * one_hot, axis=1)
    position = chosen * capacity + slot_index
    source_row = jnp.arange(row_count * fanout, dtype=jnp.int32) // fanout
    slot_table = jnp.full((experts * capacity,), row_count, jnp.int32).at[position].set(source_row)
    padded = jnp.concatenate([normed, jnp.zeros((1, normed.shape[1]), jnp.bfloat16)], axis=0)
    outgoing = padded[slot_table].reshape(experts, capacity, -1)
    arrived = lax.all_to_all(outgoing, ("sp", "tp"), split_axis=0, concat_axis=0, tiled=True)
    flat_rows = arrived.reshape(-1, arrived.shape[-1])
    hidden = (
        jax.nn.silu(jnp.dot(flat_rows, routed_gate_weight[0], preferred_element_type=jnp.float32))
        * jnp.dot(flat_rows, routed_up_weight[0], preferred_element_type=jnp.float32)
    ).astype(jnp.bfloat16)
    returned = lax.all_to_all(
        jnp.dot(hidden, routed_down_weight[0], preferred_element_type=jnp.float32)
        .astype(jnp.bfloat16)
        .reshape(arrived.shape),
        ("sp", "tp"),
        split_axis=0,
        concat_axis=0,
        tiled=True,
    )
    gathered = returned.reshape(experts * capacity, -1)[position].reshape(row_count, fanout, -1)
    routed = widened + shared
    for column in range(fanout):
        routed = routed + chosen_expert_weight[:, column, None] * gathered[:, column].astype(
            jnp.float32
        )
    return routed.astype(jnp.bfloat16)


def solution(mesh):
    in_specs = (
        P(("sp", "tp"), None),
        P("sp", "tp"),
        P("sp", "tp"),
        P("sp", "tp"),
        P("sp", "tp"),
        P("sp", "tp"),
        P("sp", "tp"),
        P(None, "tp"),
        P(None, "tp"),
        P(None, "tp"),
        P("tp"),
        P("tp"),
        P("tp"),
        P("tp"),
        P("tp", None),
        P(),
        P(("sp", "tp"), None),
        P(("sp", "tp"), None),
        P(("sp", "tp"), None, None),
        P(("sp", "tp"), None, None),
        P(("sp", "tp"), None, None),
        P(),
        P(),
        P(),
    )
    out_specs = P(("sp", "tp"), None)
    return jax.shard_map(
        on_device, mesh=mesh, in_specs=in_specs, out_specs=out_specs, check_vma=False
    )
```

profile of v0, /device:TPU:0, one launch (start us, length us, event | category | flops | bytes accessed | tf_op | source)
XLA Modules:
  0.0 401.1 jit_solution(7069635437455943211)
XLA Ops:
  8.3 5.6 %collective-permute-start.2 = (bf16[3,1024]{0,1:T(8,128)(2,1)}, bf16[3,1024]{0,1:T(8,128)(2,1)}, u32[]{:S(2)}, u32[]{:S(2)}) collective-permute-start(bf16[3,1024]{0,1:T(8,128)(2,1)} %copy.62), channel_id=1, source_target_pairs={{0,2},{2,4},{4,6},{6,8},{8,10},{10,12},{12,14},{14,16},{16,18},{18... | collective-permute-start | bytes 18440 | tf_op jit(solution)/shard_map/ppermute | solution.py:17
  14.6 2.7 collective-permute-start.1
  21.2 1.2 copy.63
  24.6 1.4 maximum_convert_fusion
  26.0 2.4 divide_multiply_fusion
  28.4 2.8 reshape.130
  31.2 2.9 broadcast_multiply_fusion
  36.2 4.7 %fusion.50 = f32[2,8,1,64,128]{4,2,3,1,0:T(1,128)} fusion(f32[2,2,8,1,1]{0,3,4,2,1:T(1,128)S(1)} %copy.85, f32[2,2,8,64,128]{4,3,2,1,0:T(8,128)S(1)} %fusion.43), kind=kOutput, calls=%fused_computation.73 | convolution fusion | flops 3145728 | bytes 1572992 | tf_op jit(solution)/shard_map/bgepn,bge->gepn/dot_general | solution.py:117
  41.6 3.4 collective-permute-start
  45.3 1.3 convert_multiply_fusion.2
  47.7 2.8 reshape.132
  50.6 38.0 %all_gather.10 = f32[16,2,8]{2,1,0:T(2,128)S(1)} all-gather(f32[1,2,8]{2,1,0:T(2,128)S(1)} %get-tuple-element.193), channel_id=1, replica_groups=mesh['sp'=16,'tp'=2] {'sp'}, dimensions={0}, use_global_device_ids=true | all-gather | bytes 1088 | tf_op jit(solution)/shard_map/all_gather | solution.py:22
  90.6 2.3 fusion.63
  93.0 60.8 %all-gather.3.cloned.1.call-done = f32[32,8,64,128]{3,2,1,0:T(8,128)} async-done(((f32[2,8,64,128]{3,2,1,0:T(8,128)}), f32[32,8,64,128]{3,2,1,0:T(8,128)}) %all-gather.3.cloned.1.call-update) | async-done | bytes 8388624 | tf_op jit(solution)/shard_map/all_gather | solution.py:22
  153.8 18.1 %while.27 = (s32[]{:T(128)}, f32[2,8,64,128]{3,2,1,0:T(8,128)S(1)}, s32[]{:T(128)}, f32[16,2,8]{2,1,0:T(2,128)S(1)}, f32[16,2,8,64,128]{4,3,2,1,0:T(8,128)}, /*index=5*/s32[]{:T(128)}, s32[]{:T(128)}) while((s32[]{:T(128)}, f32[2,8,64,128]{3,2,1,0:T(8,128)S(1)}, s32[]{:T(128)}, f32[16,2,8]{2,1,0:T(2,128)S(1)}, ...), condition=%wide.region_3.4_spmd.clone, body=%wide.region_2.3_spmd.clone.sunk | while | flops 524292 | bytes 1573161 | solution.py:31
  155.0 1.2 fusion.107
  156.2 1.2 fusion.107
  157.4 1.2 fusion.107
  158.6 1.2 fusion.107
  159.8 1.2 fusion.107
  161.0 1.2 fusion.107
  162.2 1.2 fusion.107
  163.5 1.2 fusion.107
  165.9 1.2 fusion.107
  167.1 1.2 fusion.107
  170.7 1.2 fusion.107
  171.9 4.1 %while.26 = (s32[]{:T(128)}, f32[2,8,64,128]{3,2,1,0:T(8,128)S(1)}, f32[2,2,8,64,128]{4,3,2,1,0:T(8,128)}, f32[2,2,8]{2,1,0:T(2,128)S(1)}, f32[2,2,8,64,128]{4,3,2,1,0:T(8,128)}, /*index=5*/s32[]{:T(128)}) while((s32[]{:T(128)}, f32[2,8,64,128]{3,2,1,0:T(8,128)S(1)}, f32[2,2,8,64,128]{4,3,2,1,0:T(8,128)}, f32[2,2,8]{2,1,0:T(2,128)S(1)}, ...), condition=%wide.region_5.6_spmd, body=%wide.region_4.5_spmd.sunk | while | flops 262146 | bytes 2622221 | solution.py:123
  172.8 1.2 bitcast_add_fusion.3
  174.9 1.2 bitcast_add_fusion.3
  176.1 2.4 fusion.24
  178.6 5.3 %fusion.42 = (f32[2,128,2]{1,2,0:T(2,128)S(1)}, f32[2,128,2,8,64]{1,4,3,2,0:T(8,128)S(1)}) fusion(f32[2,128,2,8,64]{1,0,4,3,2:T(2,128)} %reshape.132, f32[2,128,2,8,64]{1,0,4,3,2:T(2,128)S(1)} %copy-done.2, f32[2,8]{1,0:T(2,128)S(1)} %mul.362, f32[2,128,2,8,64]{1,4,3,2,0:T(8,128)S(1)} %fusion.24, f32[2,128,2,8,64]{1,0,4,3,2:T(2,128)S(1)} %copy-done.3, ...), kind=kOutput, calls=%fused_computation.62 | convolution fusion | flops 405798400 | bytes 5539904 | tf_op jit(solution)/shard_map/bgts,bgets,bsgep->btgep/dot_general | solution.py:110
  186.1 2.3 convolution_convert_fusion.1
  190.5 2.4 scatter_custom_fusion
  193.0 2.1 reduce-scatter.2.cloned.1.call-done
  195.1 1.3 fusion.32
  196.4 1.3 fusion.34
  197.7 4.2 %gather_fusion = bf16[768,2048]{1,0:T(8,128)(2,1)} fusion(bf16[129,2048]{1,0:T(8,128)(2,1)S(1)} %concatenate.15, s32[1024]{0:T(1024)S(1)} %pad_clamp_fusion.1), kind=kCustom, calls=%fused_computation | custom fusion | bytes 6294528 | tf_op jit(solution)/shard_map/gather | solution.py:167
  202.0 77.0 %all_to_all.10 = bf16[32,24,2048]{2,1,0:T(8,128)(2,1)S(1)} all-to-all(bf16[32,24,2048]{2,1,0:T(8,128)(2,1)} %bitcast.161), channel_id=1, replica_groups=mesh['sp'=16,'tp'=2] {'sp','tp'}, dimensions={0} | all-to-all | bytes 6291456 | tf_op jit(solution)/shard_map/all_to_all | solution.py:168
  279.0 1.7 copy-done.4
  280.6 2.9 fusion.9
  283.6 8.1 %convolution_convert_fusion = bf16[768,2048]{1,0:T(8,128)(2,1)} fusion(bf16[1,512,2048]{2,1,0:T(8,128)(2,1)S(1)} %copy-done, f32[768,512]{1,0:T(8,128)} %fusion.9, bf16[768,2048]{1,0:T(8,128)(2,1)} %bitcast.165, bf16[1,2048,512]{2,1,0:T(8,128)(2,1)} %param.47), kind=kOutput, calls=%fused_computation.9 | convolution fusion | flops 3225157632 | bytes 12058624 | tf_op jit(solution)/shard_map/dot_general | solution.py:175
  291.7 3.8 all-to-all-start.1
  295.5 2.0 fusion.93
  297.6 69.2 %all-to-all-done.1 = bf16[32,24,2048]{2,1,0:T(8,128)(2,1)} async-done(((bf16[32,24,2048]{2,1,0:T(8,128)(2,1)}), bf16[32,24,2048]{2,1,0:T(8,128)(2,1)}, u32[]{:S(2)}, u32[]{:S(2)}) %all-to-all-start.1) | async-done | bytes 3145760 | tf_op jit(solution)/shard_map/all_to_all | solution.py:174
  366.8 7.6 %gather_fusion.1 = bf16[512,2048]{1,0:T(8,128)(2,1)} fusion(bf16[768,2048]{1,0:T(8,128)(2,1)} %bitcast.40, s32[1024]{0:T(1024)S(1)} %pad_clamp_fusion), kind=kCustom, calls=%fused_computation.1 | custom fusion | bytes 4196352 | tf_op jit(solution)/shard_map/gather | solution.py:183
  374.4 4.1 %reshape.138 = bf16[128,4,2048]{2,1,0:T(4,128)(2,1)} reshape(bf16[512,2048]{1,0:T(8,128)(2,1)} %gather_fusion.1) | data formatting | bytes 4194304 | tf_op jit(solution)/shard_map/reshape | solution.py:183
  378.5 9.4 %fusion.87 = (bf16[128,1,2048]{2,1,0:T(2,128)(2,1)}, bf16[128,1,2048]{2,1,0:T(2,128)(2,1)}, bf16[128,1,2048]{2,1,0:T(2,128)(2,1)}, bf16[128,1,2048]{2,1,0:T(2,128)(2,1)}) fusion(bf16[128,4,2048]{2,1,0:T(4,128)(2,1)} %reshape.138), kind=kLoop, calls=%fused_computation.155 | loop fusion | bytes 4194304 | tf_op jit(solution)/shard_map/slice | solution.py:186
  387.9 6.4 %fusion.5 = bf16[128,2048]{1,0:T(8,128)(2,1)} fusion(bf16[512,2048]{1,0:T(8,128)(2,1)} %param.51, bf16[128,2048]{1,0:T(8,128)(2,1)S(1)} %fusion.34, bf16[2048,512]{1,0:T(8,128)(2,1)} %param.50, bf16[128,1,2048]{2,1,0:T(2,128)(2,1)} %get-tuple-element.171, bf16[128,1,2048]{2,1,0:T(2,128)(2,1)} %get-tuple-element.169, ...), kind=kOutput, calls=%fused_computation.16 | convolution fusion | flops 542244864 | bytes 8652800 | tf_op jit(solution)/shard_map/dot_general | solution.py:154
  (125 shorter events, 25.7 us)
Async XLA Ops:
  6.5 277.0 %copy-start = (bf16[1,512,2048]{2,1,0:T(8,128)(2,1)S(1)}, bf16[1,512,2048]{2,1,0:T(8,128)(2,1)}, u32[]{:S(2)}) copy-start(bf16[1,512,2048]{2,1,0:T(8,128)(2,1)} %param.48) | copy-start | bytes 6291460
  6.5 16.1 %copy-start.10 = (bf16[256,256]{1,0:T(8,128)(2,1)S(1)}, bf16[256,256]{1,0:T(8,128)(2,1)}, u32[]{:S(2)}) copy-start(bf16[256,256]{1,0:T(8,128)(2,1)} %param.30) | copy-start | bytes 393220
  6.5 147.2 %all-gather.3.cloned.1.call-start = ((), (), s32[]{:S(2)}) async-start(), calls=%async_computation.4 | async-start | bytes 8912896 | tf_op jit(solution)/shard_map/all_gather | solution.py:22
  8.3 16.3 %collective-permute-start.2 = (bf16[3,1024]{0,1:T(8,128)(2,1)}, bf16[3,1024]{0,1:T(8,128)(2,1)}, u32[]{:S(2)}, u32[]{:S(2)}) collective-permute-start(bf16[3,1024]{0,1:T(8,128)(2,1)} %copy.62), channel_id=1, source_target_pairs={{0,2},{2,4},{4,6},{6,8},{8,10},{10,12},{12,14},{14,16},{16,18},{18... | collective-permute-start | bytes 18440 | tf_op jit(solution)/shard_map/ppermute | solution.py:17
  14.6 8.0 %collective-permute-start.1 = (bf16[3,256]{1,0:T(4,128)(2,1)S(1)}, bf16[3,256]{1,0:T(4,128)(2,1)S(1)}, u32[]{:S(2)}, u32[]{:S(2)}) collective-permute-start(bf16[3,256]{1,0:T(4,128)(2,1)S(1)} %slice.127), channel_id=1, source_target_pairs={{0,2},{2,4},{4,6},{6,8},{8,10},{10,12},{12,14},{14,16},{16,18},{18... | collective-permute-start | bytes 4616 | tf_op jit(solution)/shard_map/ppermute | solution.py:17
  24.6 9.5 %copy-start.5 = (f32[2,128,2,128]{3,2,1,0:T(2,128)}, f32[2,128,2,128]{3,2,1,0:T(2,128)S(1)}, u32[]{:S(2)}) copy-start(f32[2,128,2,128]{3,2,1,0:T(2,128)S(1)} %reshape.129) | copy-start | bytes 786436
  35.2 1.0 copy-start.1
  36.2 8.9 %copy-start.9 = (bf16[256,1024]{1,0:T(8,128)(2,1)S(1)}, bf16[256,1024]{1,0:T(8,128)(2,1)}, u32[]{:S(2)}) copy-start(bf16[256,1024]{1,0:T(8,128)(2,1)} %param.32) | copy-start | bytes 1572868
  36.2 9.1 %copy-start.14 = (bf16[4,256]{1,0:T(4,128)(2,1)S(1)}, bf16[4,256]{1,0:T(4,128)(2,1)}, u32[]{:S(2)}) copy-start(bf16[4,256]{1,0:T(4,128)(2,1)} %param.37) | copy-start | bytes 6148
  40.9 154.2 %reduce-scatter.2.cloned.1.call-start = ((), (), s32[]{:S(2)}) async-start(), calls=%async_computation.3 | async-start | bytes 1572864 | tf_op jit(solution)/shard_map/reduce_scatter | solution.py:135
  41.6 47.0 %collective-permute-start = (bf16[3,256]{1,0:T(4,128)(2,1)S(1)}, bf16[3,256]{1,0:T(4,128)(2,1)S(1)}, u32[]{:S(2)}, u32[]{:S(2)}) collective-permute-start(bf16[3,256]{1,0:T(4,128)(2,1)S(1)} %slice.118), channel_id=1, source_target_pairs={{0,2},{2,4},{4,6},{6,8},{8,10},{10,12},{12,14},{14,16},{16,18},{18... | collective-permute-start | bytes 4616 | tf_op jit(solution)/shard_map/ppermute | solution.py:17
  45.3 5.3 %copy-start.19 = (f32[16]{0:T(128)S(1)}, f32[16]{0:T(128)}, u32[]{:S(2)}) copy-start(f32[16]{0:T(128)} %param.40) | copy-start | bytes 196
  47.7 40.9 %copy-start.11 = (bf16[256,256]{1,0:T(8,128)(2,1)S(1)}, bf16[256,256]{1,0:T(8,128)(2,1)}, u32[]{:S(2)}) copy-start(bf16[256,256]{1,0:T(8,128)(2,1)} %param.31) | copy-start | bytes 393220
  176.1 2.5 copy-start.2
  176.1 2.5 copy-start.3
  176.1 2.5 copy-start.8
  183.9 0.9 copy-start.15
  183.9 2.2 copy-start.17
  186.1 2.3 copy-start.13
  188.4 6.7 %copy-start.6 = (bf16[128,2048]{1,0:T(8,128)(2,1)S(1)}, bf16[128,2048]{1,0:T(8,128)(2,1)}, u32[]{:S(2)}) copy-start(bf16[128,2048]{1,0:T(8,128)(2,1)} %param.28) | copy-start | bytes 1572868
  188.4 8.0 %copy-start.12 = (f32[2048]{0:T(1024)S(1)}, f32[2048]{0:T(1024)}, u32[]{:S(2)}) copy-start(f32[2048]{0:T(1024)} %param.43) | copy-start | bytes 24580
  202.0 78.7 %copy-start.18 = (bf16[1,2048,512]{2,1,0:T(8,128)(2,1)S(1)}, bf16[1,2048,512]{2,1,0:T(8,128)(2,1)}, u32[]{:S(2)}) copy-start(bf16[1,2048,512]{2,1,0:T(8,128)(2,1)} %param.46) | copy-start | bytes 6291460
  279.0 1.7 copy-start.4
  291.7 3.8 copy-start.16
  291.7 75.1 %all-to-all-start.1 = ((bf16[32,24,2048]{2,1,0:T(8,128)(2,1)}), bf16[32,24,2048]{2,1,0:T(8,128)(2,1)}, u32[]{:S(2)}, u32[]{:S(2)}) async-start(bf16[32,24,2048]{2,1,0:T(8,128)(2,1)} %bitcast.163), calls=%async_computation.2 | async-start | bytes 6291456 | tf_op jit(solution)/shard_map/all_to_all | solution.py:174
  378.5 9.4 %copy-start.7 = (bf16[128,2048]{1,0:T(8,128)(2,1)S(1)}, bf16[128,2048]{1,0:T(8,128)(2,1)}, u32[]{:S(2)}) copy-start(bf16[128,2048]{1,0:T(8,128)(2,1)} %param.28) | copy-start | bytes 1572868
Sparse Core Ops, SparseCore 0:
  41.0 112.7 all-gather.2
  188.5 6.5 reduce-scatter.1
where the time goes:
time: 403 us; the launch traced here: 401 us
  waiting for transfers between devices  132 us (33%)
  blocking collectives  115 us (29%)
  local copies, waits for them, and re-layouts  50.6 us (13%)
  matrix products  37.5 us (9%)
  other arithmetic  36 us (9%)
  starting transfers between devices  15.5 us (4%)
  between operations  13.9 us (3%)
    all_to_all x1, blocking collectives, on_device(): lax.all_to_all(outgoing, ('sp', 'tp'), split_axis=0, concat_axis=0, tiled...  77 us
    all_to_all x1, waiting for transfers between devices, on_device(): lax.all_to_all(jnp.dot(hidden, routed_down_weight[0], preferred_element_t...  69.2 us
    all_gather x1, waiting for transfers between devices, carried_in(): pieces = jax.tree.map(lambda part: lax.all_gather(part, axis), value)  60.8 us
    all_gather x1, blocking collectives, carried_in(): pieces = jax.tree.map(lambda part: lax.all_gather(part, axis), value)  38 us
    select_n x15, other arithmetic, lap(): jnp.where(position < mine, new, old)  17.6 us
    ppermute x3, starting transfers between devices, from_behind(): return lax.ppermute(block, axis, route)  11.6 us
    slice x1, local copies, waits for them, and re-layouts, on_device(): gathered[:, column].astype(jnp.float32)  9.42 us
    dot_general x1, matrix products, on_device(): jnp.dot(hidden, routed_down_weight[0], preferred_element_type=jnp.float32)  8.11 us
  transfers between devices with their start and end apart: 6, of which 3 were waited for; matrix products, arithmetic and copies ran while one was open for 6% of the time, Pallas kernels for 0%

commit v1 on v0

--- a/solution.py
+++ b/solution.py
@@ -8,27 +8,43 @@
 BLK = 128
 
 
-precise = lax.Precision.HIGHEST
-
-
 def from_behind(block, axis, distance):
     devices = range(lax.axis_size(axis))
     route = [(i - distance, i) for i in devices if i - distance in devices]
     return lax.ppermute(block, axis, route)
 
 
-def carried_in(value, axis, join, neutral):
-    count, mine = (lax.axis_size(axis), lax.axis_index(axis))
-    pieces = jax.tree.map(lambda part: lax.all_gather(part, axis), value)
-    subtotal = jax.tree.map(
-        lambda part, zero: jnp.full_like(part, 0) + jnp.asarray(zero, part.dtype), value, neutral
-    )
-
-    def lap(position, subtotal):
-        longer = join(subtotal, jax.tree.map(lambda part: part[position], pieces))
-        return jax.tree.map(lambda new, old: jnp.where(position < mine, new, old), longer, subtotal)
-
-    return lax.fori_loop(0, count - 1, lap, subtotal)
+def swap(block, axis, step, upward_only):
+    devices = range(lax.axis_size(axis))
+    route = [(i, i ^ step) for i in devices if not (upward_only and i & step)]
+    return lax.ppermute(block, axis, route)
+
+
+def carried_in(log_total, state, axis):
+    count, mine = lax.axis_size(axis), lax.axis_index(axis)
+    heads, width = log_total.size, state.shape[-1]
+    flat = state.reshape(heads, -1, width)
+    decay = jnp.exp(log_total).reshape(heads)
+    total, before, before_decay = flat, jnp.zeros_like(flat), jnp.ones_like(decay)
+    step = 1
+    while step < count:
+        coarse = lax.reduce_precision(decay, 8, 7)
+        lane = jnp.arange(width)[None, :]
+        tail = jnp.where(lane == 0, coarse[:, None], jnp.where(lane == 1, (decay - coarse)[:, None], 0.0))
+        sent = jnp.concatenate([total.reshape(-1, width), tail], axis=0).astype(jnp.bfloat16)
+        got = swap(sent, axis, step, 2 * step >= count).astype(jnp.float32)
+        other = got[: got.shape[0] - heads].reshape(flat.shape)
+        other_decay = got[got.shape[0] - heads :, 0] + got[got.shape[0] - heads :, 1]
+        upper = (mine & step) != 0
+        before = before + jnp.where(upper, before_decay, 0.0)[:, None, None] * other
+        if 2 * step < count:
+            before_decay = before_decay * jnp.where(upper, other_decay, 1.0)
+            total = jnp.where(
+                upper, other * decay[:, None, None] + total, total * other_decay[:, None, None] + other
+            )
+            decay = decay * other_decay
+        step *= 2
+    return before.reshape(state.shape)
 
 
 def causal_conv(previous, current, weight):
@@ -42,13 +58,10 @@
     return jax.nn.silu(summed_taps)
 
 
-def combine(earlier, latter):
-    return (earlier[0] * latter[0], earlier[1] * latter[0][..., None, None] + latter[1])
-
-
-def advance(carry_state, inputs):
-    block_piece, decay_factor = inputs
-    return (carry_state * decay_factor[..., None, None] + block_piece, carry_state)
+def product(spec, *operands):
+    return jnp.einsum(
+        spec, *[part.astype(jnp.bfloat16) for part in operands], preferred_element_type=jnp.float32
+    )
 
 
 def on_device(
@@ -83,12 +96,13 @@
     groups = write_input_vectors.shape[1] // STATE
     per_group = head_count // groups
     blocks = length // BLK
-    rim_rows = (
-        head_input_signal[length - margin :],
-        write_input_vectors[length - margin :],
-        read_input_vectors[length - margin :],
-    )
-    before = from_behind((rim_rows[0], rim_rows[1], rim_rows[2]), "sp", 1)
+    wide, narrow = head_input_signal.shape[1], write_input_vectors.shape[1]
+    rim = jnp.concatenate(
+        [part[length - margin :] for part in (head_input_signal, write_input_vectors, read_input_vectors)],
+        axis=1,
+    )
+    rim = from_behind(rim, "sp", 1)
+    before = (rim[:, :wide], rim[:, wide : wide + narrow], rim[:, wide + narrow :])
     signal = causal_conv(before[0], head_input_signal, signal_filter_taps)
     write_vec = causal_conv(before[1], write_input_vectors, write_filter_taps)
     read_vec = causal_conv(before[2], read_input_vectors, read_filter_taps)
@@ -106,23 +120,26 @@
     cum_heads = jnp.transpose(within_cum, (0, 2, 3, 1))
     differences = cum_heads[..., :, None] - cum_heads[..., None, :]
     decay_matrix = jnp.exp(jnp.where(causal, differences, -jnp.inf))
-    intersection = jnp.einsum("btgn,bsgn->bgts", read_blocks, write_blocks, precision=precise)
-    intra_out = jnp.einsum(
-        "bgts,bgets,bsgep->btgep", intersection, decay_matrix, scaled_blocks, precision=precise
-    )
     tail_decay = jnp.exp(block_total[:, None] - within_cum)
-    block_states = jnp.einsum(
-        "bsgn,bsge,bsgep->bgepn", write_blocks, tail_decay, scaled_blocks, precision=precise
-    )
-    device_state = jnp.einsum(
-        "bgepn,bge->gepn", block_states, jnp.exp(device_total[None] - running), precision=precise
-    )
-    identity = (jnp.ones_like(device_total), jnp.zeros_like(device_state))
-    incoming = carried_in((jnp.exp(device_total), device_state), "sp", combine, identity)[1]
+    block_states = product(
+        "bsgn,bsgep->bgepn", write_blocks, scaled_blocks * tail_decay[..., None]
+    )
+    device_state = jnp.sum(
+        block_states * jnp.exp(device_total[None] - running)[..., None, None], axis=0
+    )
+    incoming = carried_in(device_total, device_state, "sp")
+    intersection = product("btgn,bsgn->bgts", read_blocks, write_blocks)
+    intra_out = product(
+        "bgets,bsgep->btgep", intersection[:, :, None] * decay_matrix, scaled_blocks
+    )
     readout_scale = jnp.exp(within_cum)
-    start_states = lax.scan(advance, incoming, (block_states, jnp.exp(block_total)))[1]
-    near_out = jnp.einsum(
-        "btgn,bgepn,btge->btgep", read_blocks, start_states, readout_scale, precision=precise
+    starts = [incoming]
+    for block in range(blocks - 1):
+        starts.append(
+            starts[-1] * jnp.exp(block_total[block])[..., None, None] + block_states[block]
+        )
+    near_out = (
+        product("btgn,bgepn->btgep", read_blocks, jnp.stack(starts)) * readout_scale[..., None]
     )
     ssd_out = intra_out + near_out
     ssd_out = ssd_out + head_direct_term.reshape(groups, per_group)[:, :, None] * signal_heads
@@ -157,14 +174,17 @@
     experts = sp_count * tp_count
     fanout = chosen_expert_index.shape[1]
     capacity = max(2, (3 * row_count * fanout + 2 * experts - 1) // (2 * experts))
-    chosen = chosen_expert_index.reshape(-1)
-    one_hot = (chosen[:, None] == jnp.arange(experts, dtype=jnp.int32)[None, :]).astype(jnp.int32)
-    slot_index = jnp.sum((jnp.cumsum(one_hot, axis=0) - one_hot) * one_hot, axis=1)
-    position = chosen * capacity + slot_index
-    source_row = jnp.arange(row_count * fanout, dtype=jnp.int32) // fanout
-    slot_table = jnp.full((experts * capacity,), row_count, jnp.int32).at[position].set(source_row)
-    padded = jnp.concatenate([normed, jnp.zeros((1, normed.shape[1]), jnp.bfloat16)], axis=0)
-    outgoing = padded[slot_table].reshape(experts, capacity, -1)
+    named = chosen_expert_index[:, :, None] == jnp.arange(experts, dtype=jnp.int32)
+    hits = jnp.any(named, axis=1)
+    share = jnp.sum(jnp.where(named, chosen_expert_weight[:, :, None], 0.0), axis=1)
+    ahead = (jnp.arange(row_count)[:, None] > jnp.arange(row_count)[None, :]).astype(jnp.bfloat16)
+    slot = jnp.dot(ahead, hits.astype(jnp.bfloat16), preferred_element_type=jnp.float32)
+    slot = jnp.where(hits, slot.astype(jnp.int32), -1)
+    places = jnp.arange(capacity, dtype=jnp.int32)
+    pick = (slot.T[:, None, :] == places[None, :, None]).reshape(experts * capacity, row_count)
+    outgoing = jnp.dot(
+        pick.astype(jnp.bfloat16), normed, preferred_element_type=jnp.float32
+    ).astype(jnp.bfloat16).reshape(experts, capacity, -1)
     arrived = lax.all_to_all(outgoing, ("sp", "tp"), split_axis=0, concat_axis=0, tiled=True)
     flat_rows = arrived.reshape(-1, arrived.shape[-1])
     hidden = (
@@ -180,13 +200,14 @@
         concat_axis=0,
         tiled=True,
     )
-    gathered = returned.reshape(experts * capacity, -1)[position].reshape(row_count, fanout, -1)
-    routed = widened + shared
-    for column in range(fanout):
-        routed = routed + chosen_expert_weight[:, column, None] * gathered[:, column].astype(
-            jnp.float32
-        )
-    return routed.astype(jnp.bfloat16)
+    spread = jnp.where(slot[:, :, None] == places, share[:, :, None], 0.0)
+    spread = spread.reshape(row_count, experts * capacity)
+    coarse = lax.reduce_precision(spread, 8, 7)
+    back = returned.reshape(experts * capacity, -1)
+    routed = jnp.dot(
+        coarse.astype(jnp.bfloat16), back, preferred_element_type=jnp.float32
+    ) + jnp.dot((spread - coarse).astype(jnp.bfloat16), back, preferred_element_type=jnp.float32)
+    return (widened + shared + routed).astype(jnp.bfloat16)
 
 
 def solution(mesh):

time: 403 us -> 313 us (0.78)
  waiting for transfers between devices: 132 us -> 83.6 us
  blocking collectives: 115 us -> 76.8 us
  local copies, waits for them, and re-layouts: 50.6 us -> 45.3 us
  starting transfers between devices: 15.5 us -> 20.4 us
    all_gather x1 -> x0, waiting for transfers between devices: 60.8 us -> none  [carried_in(): pieces = jax.tree.map(lambda part: lax.all_gather(part, axis), value)]
    all_gather x1 -> x0, blocking collectives: 38 us -> none  [carried_in(): pieces = jax.tree.map(lambda part: lax.all_gather(part, axis), value)]
    select_n x18 -> x1, other arithmetic: 17.6 us -> 1.49 us  [carried_in(): before = before + jnp.where(upper, before_decay, 0.0)[:, None, None] * other]
    gather x2 -> x0, local copies, waits for them, and re-layouts: 11.8 us -> none  [the longest x1 7.56 us: on_device(): returned.reshape(experts * capacity, -1)[position]]
    ppermute x0 -> x4, starting transfers between devices: none -> 10.8 us  [swap(): return lax.ppermute(block, axis, route)]
    reduce_scatter x1, waiting for transfers between devices: 2.08 us -> 11.8 us  [on_device(): lax.psum_scatter(jnp.dot(mixer_out, mixer_output_weight, preferred_elemen...]
    another operation x2 -> x10, other arithmetic: 1.2 us -> 10.4 us
    mul x21 -> x12, local copies, waits for them, and re-layouts: 0.36 us -> 8.89 us  [the longest x6 4.71 us: carried_in(): other * decay[:, None, None] + total]
  transfers between devices with their start and end apart: 6 -> 7, of which waited for: 3 -> 4; matrix products, arithmetic and copies ran while one was open for 6% -> 12% of each run, Pallas kernels for 0% -> 0%
where the time goes in v1:
time: 313 us; the launch traced here: 312 us
  waiting for transfers between devices  83.6 us (27%)
  blocking collectives  76.8 us (25%)
  local copies, waits for them, and re-layouts  45.3 us (14%)
  other arithmetic  35.9 us (11%)
  matrix products  35.8 us (11%)
  starting transfers between devices  20.4 us (7%)
  between operations  13.9 us (4%)
    all_to_all x1, blocking collectives, on_device(): lax.all_to_all(outgoing, ('sp', 'tp'), split_axis=0, concat_axis=0, tiled...  76.8 us
    all_to_all x1, waiting for transfers between devices, on_device(): lax.all_to_all(jnp.dot(hidden, routed_down_weight[0], preferred_element_t...  69.1 us
    reduce_scatter x1, waiting for transfers between devices, on_device(): lax.psum_scatter(jnp.dot(mixer_out, mixer_output_weight, preferred_elemen...  11.8 us
    ppermute x4, starting transfers between devices, swap(): return lax.ppermute(block, axis, route)  10.8 us
    another operation x10, other arithmetic  10.4 us
    unnamed x60, local copies, waits for them, and re-layouts  9.52 us
    dot_general x1, matrix products, on_device(): jnp.dot(hidden, routed_down_weight[0], preferred_element_type=jnp.float32)  8.14 us
  transfers between devices with their start and end apart: 7, of which 4 were waited for; matrix products, arithmetic and copies ran while one was open for 12% of the time, Pallas kernels for 0%

profile of v1, /device:TPU:0, one launch (start us, length us, event | category | flops | bytes accessed | tf_op | source)
XLA Modules:
  0.0 311.6 jit_solution(11151642979809105203)
XLA Ops:
  9.8 5.6 %collective-permute-start = (bf16[3,1536]{0,1:T(8,128)(2,1)}, bf16[3,1536]{0,1:T(8,128)(2,1)}, u32[]{:S(2)}, u32[]{:S(2)}) collective-permute-start(bf16[3,1536]{0,1:T(8,128)(2,1)} %copy.138), channel_id=1, source_target_pairs={{0,2},{2,4},{4,6},{6,8},{8,10},{10,12},{12,14},{14,16},{16,18},{18... | collective-permute-start | bytes 27656 | tf_op jit(solution)/shard_map/ppermute | solution.py:14
  15.4 1.4 fusion.100
  20.0 1.2 copy.139
  22.0 1.3 collective-permute-done
  24.7 2.4 divide_multiply_fusion
  27.1 1.7 reshape.390
  28.8 1.5 fusion.120
  33.1 2.1 multiply_reduce_fusion
  36.8 2.5 collective-permute-start.1
  40.6 2.0 copy.156
  44.0 2.3 convert_multiply_fusion.2
  49.5 1.4 mul.555
  52.4 2.5 fusion.117
  55.5 1.5 collective-permute-start.2
  57.6 2.8 reshape.397
  61.8 1.6 copy.153
  64.1 1.5 copy.142
  66.5 1.0 convert_element_type.130
  69.1 1.2 fusion.115
  71.0 1.4 mul.568
  72.3 1.3 mul.563
  73.6 1.4 mul.564
  74.9 1.4 reduce-precision_reduce_fusion.1
  77.1 1.5 fusion.112
  79.4 1.6 collective-permute-start.3
  81.0 1.5 multiply_convert_fusion.6
  85.1 1.3 collective-permute-done.3
  88.2 1.5 select_reduce_fusion.2
  90.6 2.2 select_convert_fusion
  93.0 5.2 %collective-permute-start.4 = (bf16[1040,128]{1,0:T(8,128)(2,1)S(1)}, bf16[1040,128]{1,0:T(8,128)(2,1)}, u32[]{:S(2)}, u32[]{:S(2)}) collective-permute-start(bf16[1040,128]{1,0:T(8,128)(2,1)S(1)} %pad_maximum_fusion.3), channel_id=1, source_target_pairs={{0,16},{2,18},{4,20},{6,22},{8,24},{10,26},{12,28},{14,30},{1,17},... | collective-permute-start | bytes 798728 | tf_op jit(solution)/shard_map/ppermute | solution.py:20
  98.2 2.7 convolution_bitcast_fusion.1
  100.9 1.8 slice.211
  103.6 1.1 slice.214
  105.7 1.6 fusion.113
  109.9 2.3 convolution_convert_fusion.2
  112.6 11.8 %reduce-scatter.2.cloned.1.call-done = bf16[128,2048]{1,0:T(8,128)(2,1)} async-done(((bf16[256,2048]{1,0:T(8,128)(2,1)}), bf16[128,2048]{1,0:T(8,128)(2,1)}) %reduce-scatter.2.cloned.1.call-update) | async-done | bytes 524304 | tf_op jit(solution)/shard_map/reduce_scatter | solution.py:152
  124.4 1.5 fusion.30
  125.9 1.1 convolution_convert_fusion.1
  127.0 76.8 %all_to_all.10 = bf16[32,24,2048]{2,1,0:T(8,128)(2,1)S(1)} all-to-all(bf16[32,24,2048]{2,1,0:T(8,128)(2,1)S(1)} %bitcast.107), channel_id=1, replica_groups=mesh['sp'=16,'tp'=2] {'sp','tp'}, dimensions={0} | all-to-all | bytes 6291456 | tf_op jit(solution)/shard_map/all_to_all | solution.py:188
  203.8 1.7 copy-done.5
  205.5 3.0 fusion.18
  208.4 8.1 %convolution_convert_fusion = bf16[768,2048]{1,0:T(8,128)(2,1)} fusion(bf16[1,512,2048]{2,1,0:T(8,128)(2,1)S(1)} %copy-done, f32[768,512]{1,0:T(8,128)} %fusion.18, bf16[768,2048]{1,0:T(8,128)(2,1)} %bitcast.111, bf16[1,2048,512]{2,1,0:T(8,128)(2,1)} %param.43), kind=kOutput, calls=%fused_computation | convolution fusion | flops 3225157632 | bytes 12058624 | tf_op jit(solution)/shard_map/dot_general | solution.py:195
  216.6 4.0 %all-to-all-start.1 = ((bf16[32,24,2048]{2,1,0:T(8,128)(2,1)}), bf16[32,24,2048]{2,1,0:T(8,128)(2,1)}, u32[]{:S(2)}, u32[]{:S(2)}) async-start(bf16[32,24,2048]{2,1,0:T(8,128)(2,1)} %bitcast.109), calls=%async_computation.2 | async-start | bytes 6291456 | tf_op jit(solution)/shard_map/all_to_all | solution.py:194
  220.6 2.1 fusion.52
  222.7 69.1 %all-to-all-done.1 = bf16[32,24,2048]{2,1,0:T(8,128)(2,1)} async-done(((bf16[32,24,2048]{2,1,0:T(8,128)(2,1)}), bf16[32,24,2048]{2,1,0:T(8,128)(2,1)}, u32[]{:S(2)}, u32[]{:S(2)}) %all-to-all-start.1) | async-done | bytes 3145760 | tf_op jit(solution)/shard_map/all_to_all | solution.py:194
  291.8 3.9 %fusion.4 = f32[128,2048]{1,0:T(8,128)S(1)} fusion(bf16[32,24,2048]{2,1,0:T(8,128)(2,1)} %all-to-all-done.1, f32[128,32]{0,1:T(8,128)S(1)} %select_reduce_fusion, s32[128,32]{0,1:T(8,128)S(1)} %fusion.26), kind=kOutput, calls=%fused_computation.7 | convolution fusion | flops 403046400 | bytes 4227072 | tf_op jit(solution)/shard_map/dot_general | solution.py:207
  295.7 4.9 %fusion.11 = f32[128,2048]{1,0:T(8,128)} fusion(f32[128,2048]{1,0:T(8,128)S(1)} %fusion.4, bf16[32,24,2048]{2,1,0:T(8,128)(2,1)} %all-to-all-done.1, f32[128,32]{0,1:T(8,128)S(1)} %select_reduce_fusion, s32[128,32]{0,1:T(8,128)S(1)} %fusion.26), kind=kOutput, calls=%fused_computation.11 | convolution fusion | flops 403406848 | bytes 5275648 | tf_op jit(solution)/shard_map/dot_general | solution.py:209
  300.6 4.2 %fusion.14 = bf16[128,2048]{1,0:T(8,128)(2,1)} fusion(f32[128,2048]{1,0:T(8,128)} %fusion.11, bf16[512,2048]{1,0:T(8,128)(2,1)} %param.47, bf16[128,2048]{1,0:T(8,128)(2,1)S(1)} %get-tuple-element.18, bf16[2048,512]{1,0:T(8,128)(2,1)} %param.46, f32[2048]{0:T(1024)S(1)} %copy-done.11, f32[128]{0:T(128)S(1)} %add_rsqrt_fusion, f32[128,512]{1,0:T(8,128)S(1)} %fusion.52), kind=kOutput, calls=%fused_computation.12 | convolution fusion | flops 539361280 | bytes 6562304 | tf_op jit(solution)/shard_map/dot_general | solution.py:171
  (133 shorter events, 38.4 us)
Async XLA Ops:
  6.5 201.9 %copy-start = (bf16[1,512,2048]{2,1,0:T(8,128)(2,1)S(1)}, bf16[1,512,2048]{2,1,0:T(8,128)(2,1)}, u32[]{:S(2)}) copy-start(bf16[1,512,2048]{2,1,0:T(8,128)(2,1)} %param.44) | copy-start | bytes 6291460
  6.5 117.9 %reduce-scatter.2.cloned.1.call-start = ((), (), s32[]{:S(2)}) async-start(), calls=%async_computation.3 | async-start | bytes 1572864 | tf_op jit(solution)/shard_map/reduce_scatter | solution.py:152
  9.8 13.5 %collective-permute-start = (bf16[3,1536]{0,1:T(8,128)(2,1)}, bf16[3,1536]{0,1:T(8,128)(2,1)}, u32[]{:S(2)}, u32[]{:S(2)}) collective-permute-start(bf16[3,1536]{0,1:T(8,128)(2,1)} %copy.138), channel_id=1, source_target_pairs={{0,2},{2,4},{4,6},{6,8},{8,10},{10,12},{12,14},{14,16},{16,18},{18... | collective-permute-start | bytes 27656 | tf_op jit(solution)/shard_map/ppermute | solution.py:14
  17.1 7.5 %copy-start.14 = (pred[128]{0:T(512)(128)(4,1)}, pred[128]{0:T(512)(128)(4,1)S(1)}, u32[]{:S(2)}) copy-start(pred[128]{0:T(512)(128)(4,1)S(1)} %get-tuple-element.58) | copy-start | bytes 388
  17.2 7.5 %copy-start.15 = (pred[128]{0:T(512)(128)(4,1)}, pred[128]{0:T(512)(128)(4,1)S(1)}, u32[]{:S(2)}) copy-start(pred[128]{0:T(512)(128)(4,1)S(1)} %get-tuple-element.59) | copy-start | bytes 388
  19.9 4.8 %copy-start.20 = (f32[1,2,8]{2,1,0:T(2,128)}, f32[1,2,8]{2,1,0:T(2,128)S(1)}, u32[]{:S(2)}) copy-start(f32[1,2,8]{2,1,0:T(2,128)S(1)} %get-tuple-element.43) | copy-start | bytes 196
  19.9 4.7 %copy-start.23 = (f32[16]{0:T(128)}, f32[16]{0:T(128)S(1)}, u32[]{:S(2)}) copy-start(f32[16]{0:T(128)S(1)} %exp.106) | copy-start | bytes 196
  33.1 6.1 %copy-start.16 = (bf16[4,256]{1,0:T(4,128)(2,1)S(1)}, bf16[4,256]{1,0:T(4,128)(2,1)}, u32[]{:S(2)}) copy-start(bf16[4,256]{1,0:T(4,128)(2,1)} %param.33) | copy-start | bytes 6148
  35.2 0.8 copy-start.3
  36.8 9.5 %collective-permute-start.1 = (bf16[1040,128]{1,0:T(8,128)(2,1)}, bf16[1040,128]{1,0:T(8,128)(2,1)}, u32[]{:S(2)}, u32[]{:S(2)}) collective-permute-start(bf16[1040,128]{1,0:T(8,128)(2,1)} %pad_maximum_fusion), channel_id=1, source_target_pairs={{0,2},{2,0},{4,6},{6,4},{8,10},{10,8},{12,14},{14,12},{16,18},{18,... | collective-permute-start | bytes 798728 | tf_op jit(solution)/shard_map/ppermute | solution.py:20
  47.3 0.8 copy-start.8
  48.3 0.6 copy-start.17
  52.4 8.1 %copy-start.28 = (f32[16]{0:T(128)S(1)}, f32[16]{0:T(128)}, u32[]{:S(2)}) copy-start(f32[16]{0:T(128)} %param.36) | copy-start | bytes 196
  55.5 11.0 %collective-permute-start.2 = (bf16[1040,128]{1,0:T(8,128)(2,1)}, bf16[1040,128]{1,0:T(8,128)(2,1)}, u32[]{:S(2)}, u32[]{:S(2)}) collective-permute-start(bf16[1040,128]{1,0:T(8,128)(2,1)} %pad_maximum_fusion.1), channel_id=1, source_target_pairs={{0,4},{2,6},{4,0},{6,2},{8,12},{10,14},{12,8},{14,10},{16,20},{18,... | collective-permute-start | bytes 798728 | tf_op jit(solution)/shard_map/ppermute | solution.py:20
  67.5 0.8 copy-start.1
  79.4 7.0 %collective-permute-start.3 = (bf16[1040,128]{1,0:T(8,128)(2,1)}, bf16[1040,128]{1,0:T(8,128)(2,1)}, u32[]{:S(2)}, u32[]{:S(2)}) collective-permute-start(bf16[1040,128]{1,0:T(8,128)(2,1)} %pad_maximum_fusion.2), channel_id=1, source_target_pairs={{0,8},{2,10},{4,12},{6,14},{8,0},{10,2},{12,4},{14,6},{16,24},{18,... | collective-permute-start | bytes 798728 | tf_op jit(solution)/shard_map/ppermute | solution.py:20
  87.4 0.8 copy-start.7
  89.9 8.3 %copy-start.10 = (f32[2,2,128,128]{3,2,1,0:T(8,128)S(1)}, f32[2,2,128,128]{3,2,1,0:T(8,128)}, u32[]{:S(2)}) copy-start(f32[2,2,128,128]{3,2,1,0:T(8,128)} %fusion.95) | copy-start | bytes 786436
  92.9 9.8 %copy-start.25 = (f32[16]{0:T(128)S(1)}, f32[16]{0:T(128)}, u32[]{:S(2)}) copy-start(f32[16]{0:T(128)} %get-tuple-element.6) | copy-start | bytes 196
  92.9 9.8 %copy-start.24 = (f32[16]{0:T(128)S(1)}, f32[16]{0:T(128)}, u32[]{:S(2)}) copy-start(f32[16]{0:T(128)} %get-tuple-element.5) | copy-start | bytes 196
  93.0 11.7 %collective-permute-start.4 = (bf16[1040,128]{1,0:T(8,128)(2,1)S(1)}, bf16[1040,128]{1,0:T(8,128)(2,1)}, u32[]{:S(2)}, u32[]{:S(2)}) collective-permute-start(bf16[1040,128]{1,0:T(8,128)(2,1)S(1)} %pad_maximum_fusion.3), channel_id=1, source_target_pairs={{0,16},{2,18},{4,20},{6,22},{8,24},{10,26},{12,28},{14,30},{1,17},... | collective-permute-start | bytes 798728 | tf_op jit(solution)/shard_map/ppermute | solution.py:20
  103.6 3.7 %copy-start.6 = (f32[2,2,8,64,128]{4,3,2,1,0:T(8,128)S(1)}, f32[2,2,8,64,128]{4,3,2,1,0:T(8,128)}, u32[]{:S(2)}) copy-start(f32[2,2,8,64,128]{4,3,2,1,0:T(8,128)} %get-tuple-element.55) | copy-start | bytes 3145732
  103.6 3.7 %copy-start.21 = (f32[2,8]{1,0:T(2,128)S(1)}, f32[2,8]{1,0:T(2,128)}, u32[]{:S(2)}) copy-start(f32[2,8]{1,0:T(2,128)} %fusion.104) | copy-start | bytes 196
  105.6 1.8 copy-start.4
  105.6 1.8 copy-start.9
  105.6 1.8 copy-start.12
  105.7 1.8 copy-start.19
  107.5 2.4 copy-start.26
  108.0 1.3 copy-start.2
  108.0 1.3 copy-start.18
  109.9 2.4 copy-start.13
  112.1 13.8 %copy-start.11 = (f32[2048]{0:T(1024)S(1)}, f32[2048]{0:T(1024)}, u32[]{:S(2)}) copy-start(f32[2048]{0:T(1024)} %param.39) | copy-start | bytes 24580
  127.0 78.5 %copy-start.27 = (bf16[1,2048,512]{2,1,0:T(8,128)(2,1)S(1)}, bf16[1,2048,512]{2,1,0:T(8,128)(2,1)}, u32[]{:S(2)}) copy-start(bf16[1,2048,512]{2,1,0:T(8,128)(2,1)} %param.42) | copy-start | bytes 6291460
  203.8 1.7 copy-start.5
  216.6 4.0 %copy-start.22 = (f32[128,4]{0,1:T(4,128)S(1)}, f32[128,4]{0,1:T(4,128)}, u32[]{:S(2)}) copy-start(f32[128,4]{0,1:T(4,128)} %param.41) | copy-start | bytes 6148
  216.6 75.2 %all-to-all-start.1 = ((bf16[32,24,2048]{2,1,0:T(8,128)(2,1)}), bf16[32,24,2048]{2,1,0:T(8,128)(2,1)}, u32[]{:S(2)}, u32[]{:S(2)}) async-start(bf16[32,24,2048]{2,1,0:T(8,128)(2,1)} %bitcast.109), calls=%async_computation.2 | async-start | bytes 6291456 | tf_op jit(solution)/shard_map/all_to_all | solution.py:194
Sparse Core Ops, SparseCore 0:
  112.3 12.1 reduce-scatter.1

commit v2 on v1

--- a/solution.py
+++ b/solution.py
@@ -149,14 +149,21 @@
     norm_scale = lax.rsqrt(jnp.mean(gated * gated, axis=-1, keepdims=True) + 1e-06)
     mixer_out = ((gated * norm_scale).reshape(length, -1) * grouped_norm_gain).astype(jnp.bfloat16)
     row_count = stream.shape[0]
-    summed = lax.psum_scatter(
-        jnp.dot(mixer_out, mixer_output_weight, preferred_element_type=jnp.float32).astype(
-            jnp.bfloat16
-        ),
-        "tp",
-        scatter_dimension=0,
-        tiled=True,
-    ).astype(jnp.float32)
+    tp_count = lax.axis_size("tp")
+    core = lax.axis_index("tp")
+
+    def share_of(owner):
+        rows = lax.dynamic_slice_in_dim(mixer_out, owner * row_count, row_count, 0)
+        return jnp.dot(rows, mixer_output_weight, preferred_element_type=jnp.float32)
+
+    shares = []
+    for ahead in range(1, tp_count):
+        route = [(i, (i + ahead) % tp_count) for i in range(tp_count)]
+        part = share_of((core + ahead) % tp_count).astype(jnp.bfloat16)
+        shares.append(lax.ppermute(part, "tp", route))
+    summed = share_of(core)
+    for part in shares:
+        summed = summed + part.astype(jnp.float32)
     residual = (stream.astype(jnp.float32) + summed).astype(jnp.bfloat16)
     widened = residual.astype(jnp.float32)
     normed = (
@@ -170,7 +177,6 @@
     ).astype(jnp.bfloat16)
     shared = jnp.dot(shared_hidden, common_down_weight, preferred_element_type=jnp.float32)
     sp_count = lax.axis_size("sp")
-    tp_count = lax.axis_size("tp")
     experts = sp_count * tp_count
     fanout = chosen_expert_index.shape[1]
     capacity = max(2, (3 * row_count * fanout + 2 * experts - 1) // (2 * experts))
@@ -181,33 +187,66 @@
     slot = jnp.dot(ahead, hits.astype(jnp.bfloat16), preferred_element_type=jnp.float32)
     slot = jnp.where(hits, slot.astype(jnp.int32), -1)
     places = jnp.arange(capacity, dtype=jnp.int32)
-    pick = (slot.T[:, None, :] == places[None, :, None]).reshape(experts * capacity, row_count)
-    outgoing = jnp.dot(
-        pick.astype(jnp.bfloat16), normed, preferred_element_type=jnp.float32
-    ).astype(jnp.bfloat16).reshape(experts, capacity, -1)
-    arrived = lax.all_to_all(outgoing, ("sp", "tp"), split_axis=0, concat_axis=0, tiled=True)
-    flat_rows = arrived.reshape(-1, arrived.shape[-1])
-    hidden = (
-        jax.nn.silu(jnp.dot(flat_rows, routed_gate_weight[0], preferred_element_type=jnp.float32))
-        * jnp.dot(flat_rows, routed_up_weight[0], preferred_element_type=jnp.float32)
-    ).astype(jnp.bfloat16)
-    returned = lax.all_to_all(
-        jnp.dot(hidden, routed_down_weight[0], preferred_element_type=jnp.float32)
-        .astype(jnp.bfloat16)
-        .reshape(arrived.shape),
-        ("sp", "tp"),
-        split_axis=0,
-        concat_axis=0,
-        tiled=True,
-    )
-    spread = jnp.where(slot[:, :, None] == places, share[:, :, None], 0.0)
-    spread = spread.reshape(row_count, experts * capacity)
-    coarse = lax.reduce_precision(spread, 8, 7)
-    back = returned.reshape(experts * capacity, -1)
-    routed = jnp.dot(
-        coarse.astype(jnp.bfloat16), back, preferred_element_type=jnp.float32
-    ) + jnp.dot((spread - coarse).astype(jnp.bfloat16), back, preferred_element_type=jnp.float32)
-    return (widened + shared + routed).astype(jnp.bfloat16)
+    half = experts // 2
+    side = lax.axis_index("sp") // (sp_count // 2)
+    sides = [list(range(half)), list(range(half, experts))]
+    across = sp_count // 2
+    tables = jnp.stack([slot.astype(jnp.float32), share])
+    near_table = lax.dynamic_slice_in_dim(tables, side * half, half, 2)
+    far_table = swap(
+        lax.dynamic_slice_in_dim(tables, (1 - side) * half, half, 2), "sp", across, False
+    )
+
+    def exchange(block):
+        return lax.all_to_all(
+            block,
+            ("sp", "tp"),
+            split_axis=0,
+            concat_axis=0,
+            axis_index_groups=sides,
+            tiled=True,
+        )
+
+    def dispatch(table, rows):
+        slots = table[0].astype(jnp.int32)
+        pick = slots.T[:, None, :] == places[None, :, None]
+        pick = pick.reshape(half * capacity, row_count).astype(jnp.bfloat16)
+        picked = jnp.dot(pick, rows, preferred_element_type=jnp.float32)
+        return exchange(picked.astype(jnp.bfloat16).reshape(half, capacity, -1))
+
+    def expert(arrived):
+        flat_rows = arrived.reshape(half * capacity, -1)
+        hidden = (
+            jax.nn.silu(
+                jnp.dot(flat_rows, routed_gate_weight[0], preferred_element_type=jnp.float32)
+            )
+            * jnp.dot(flat_rows, routed_up_weight[0], preferred_element_type=jnp.float32)
+        ).astype(jnp.bfloat16)
+        result = jnp.dot(hidden, routed_down_weight[0], preferred_element_type=jnp.float32)
+        return result.astype(jnp.bfloat16).reshape(arrived.shape)
+
+    def collect(table, returned):
+        slots = table[0].astype(jnp.int32)
+        spread = jnp.where(slots[:, :, None] == places, table[1][:, :, None], 0.0)
+        spread = spread.reshape(row_count, half * capacity)
+        coarse = lax.reduce_precision(spread, 8, 7)
+        fine = (spread - coarse).astype(jnp.bfloat16)
+        back = returned.reshape(half * capacity, -1)
+        return jnp.dot(
+            coarse.astype(jnp.bfloat16), back, preferred_element_type=jnp.float32
+        ) + jnp.dot(fine, back, preferred_element_type=jnp.float32)
+
+    far_rows = swap(normed, "sp", across, False)
+    near_rows = dispatch(near_table, normed)
+    near_rows, far_rows = lax.optimization_barrier((near_rows, far_rows))
+    far_arrived = dispatch(far_table, far_rows)
+    near_out = expert(near_rows)
+    far_out = expert(far_arrived)
+    far_sum = collect(far_table, exchange(far_out)).astype(jnp.bfloat16)
+    near_out, far_sum = lax.optimization_barrier((near_out, far_sum))
+    from_far = swap(far_sum, "sp", across, False)
+    near_sum = collect(near_table, exchange(near_out))
+    return (widened + shared + near_sum + from_far.astype(jnp.float32)).astype(jnp.bfloat16)
 
 
 def solution(mesh):

time: 313 us -> 272 us (0.87)
  blocking collectives: 76.8 us -> 26.4 us
  starting transfers between devices: 20.4 us -> 36.7 us
  between operations: 13.9 us -> 0.58 us
  matrix products: 35.8 us -> 46.7 us
  waiting for transfers between devices: 83.6 us -> 78.6 us
    all_to_all x1, blocking collectives: 76.8 us -> 26.4 us  [exchange(): lax.all_to_all(block, ('sp', 'tp'), split_axis=0, concat_axis=0, axis_ind...]
    ppermute x4 -> x7, waiting for transfers between devices: 1.33 us -> 32 us  [swap(): return lax.ppermute(block, axis, route)]
    all_to_all x1 -> x3, waiting for transfers between devices: 69.1 us -> 46.6 us  [exchange(): lax.all_to_all(block, ('sp', 'tp'), split_axis=0, concat_axis=0, axis_ind...]
    all_to_all x1 -> x3, starting transfers between devices: 4 us -> 15.9 us  [exchange(): lax.all_to_all(block, ('sp', 'tp'), split_axis=0, concat_axis=0, axis_ind...]
    reduce_scatter x1 -> x0, waiting for transfers between devices: 11.8 us -> none  [on_device(): lax.psum_scatter(jnp.dot(mixer_out, mixer_output_weight, preferred_elemen...]
    dot_general x6 -> x12, matrix products: 23.2 us -> 33.2 us  [the longest x2 10.6 us: expert(): jnp.dot(hidden, routed_down_weight[0], preferred_element_type=jnp.float32)]
    ppermute x4 -> x7, starting transfers between devices: 10.8 us -> 15 us  [swap(): return lax.ppermute(block, axis, route)]
    another operation x10 -> x11, other arithmetic: 10.4 us -> 9.69 us
  transfers between devices with their start and end apart: 7 -> 12, of which waited for: 4 -> 6; matrix products, arithmetic and copies ran while one was open for 12% -> 19% of each run, Pallas kernels for 0% -> 0%
where the time goes in v2:
time: 272 us; the launch traced here: 270 us
  waiting for transfers between devices  78.6 us (29%)
  matrix products  46.7 us (17%)
  local copies, waits for them, and re-layouts  45.5 us (17%)
  starting transfers between devices  36.7 us (13%)
  other arithmetic  35.7 us (13%)
  blocking collectives  26.4 us (10%)
    all_to_all x3, waiting for transfers between devices, exchange(): lax.all_to_all(block, ('sp', 'tp'), split_axis=0, concat_axis=0, axis_ind...  46.6 us
    ppermute x7, waiting for transfers between devices, swap(): return lax.ppermute(block, axis, route)  32 us
    all_to_all x1, blocking collectives, exchange(): lax.all_to_all(block, ('sp', 'tp'), split_axis=0, concat_axis=0, axis_ind...  26.4 us
    all_to_all x3, starting transfers between devices, exchange(): lax.all_to_all(block, ('sp', 'tp'), split_axis=0, concat_axis=0, axis_ind...  15.9 us
    ppermute x7, starting transfers between devices, swap(): return lax.ppermute(block, axis, route)  15 us
    dot_general x2, matrix products, expert(): jnp.dot(hidden, routed_down_weight[0], preferred_element_type=jnp.float32)  10.6 us
    unnamed x76, local copies, waits for them, and re-layouts  9.89 us
    another operation x10, other arithmetic  9.68 us
  transfers between devices with their start and end apart: 12, of which 6 were waited for; matrix products, arithmetic and copies ran while one was open for 19% of the time, Pallas kernels for 0%

profile of v2, /device:TPU:0, one launch (start us, length us, event | category | flops | bytes accessed | tf_op | source)
XLA Modules:
  0.0 270.2 jit_solution(17647930401037355570)
XLA Ops:
  3.2 5.6 %collective-permute-start = (bf16[3,1536]{0,1:T(8,128)(2,1)}, bf16[3,1536]{0,1:T(8,128)(2,1)}, u32[]{:S(2)}, u32[]{:S(2)}) collective-permute-start(bf16[3,1536]{0,1:T(8,128)(2,1)} %copy.131), channel_id=1, source_target_pairs={{0,2},{2,4},{4,6},{6,8},{8,10},{10,12},{12,14},{14,16},{16,18},{18... | collective-permute-start | bytes 27656 | tf_op jit(solution)/shard_map/ppermute | solution.py:14
  8.9 1.4 fusion.124
  18.6 2.4 divide_multiply_fusion
  21.0 1.7 reshape.432
  22.7 1.5 fusion.158
  27.1 2.1 multiply_reduce_fusion
  30.7 2.0 collective-permute-start.1
  35.6 2.0 copy.149
  37.6 2.3 convert_multiply_fusion.2
  45.9 2.5 fusion.155
  49.1 1.5 collective-permute-start.2
  51.9 1.7 copy.146
  53.6 2.7 %reshape.439 = f32[2,128,2,8,64]{1,0,4,3,2:T(2,128)} reshape(f32[256,1024]{0,1:T(8,128)} %convert_multiply_fusion.2) | data formatting | bytes 2097152 | tf_op jit(solution)/shard_map/reshape | solution.py:148
  65.6 1.4 mul.582
  68.3 1.4 mul.586
  69.7 1.4 reduce-precision_reduce_fusion.1
  71.8 1.5 fusion.145
  74.1 1.6 collective-permute-start.3
  75.7 1.5 multiply_convert_fusion.5
  83.0 1.5 select_reduce_fusion.2
  84.6 2.3 select_convert_fusion
  87.0 5.2 %collective-permute-start.4 = (bf16[1040,128]{1,0:T(8,128)(2,1)S(1)}, bf16[1040,128]{1,0:T(8,128)(2,1)}, u32[]{:S(2)}, u32[]{:S(2)}) collective-permute-start(bf16[1040,128]{1,0:T(8,128)(2,1)S(1)} %pad_maximum_fusion.3), channel_id=1, source_target_pairs={{0,16},{2,18},{4,20},{6,22},{8,24},{10,26},{12,28},{14,30},{1,17},... | collective-permute-start | bytes 798728 | tf_op jit(solution)/shard_map/ppermute | solution.py:20
  92.2 2.7 convolution_bitcast_fusion.5
  94.9 1.8 slice.229
  99.6 1.6 fusion.151
  105.7 4.2 %collective-permute-done.7 = f32[2,128,16]{1,2,0:T(8,128)S(1)} collective-permute-done((f32[2,128,16]{1,2,0:T(8,128)S(1)}, f32[2,128,16]{1,2,0:T(8,128)S(1)}, u32[]{:S(2)}, u32[]{:S(2)}) %collective-permute-start.7) | collective-permute-done | bytes 16416 | tf_op jit(solution)/shard_map/ppermute | solution.py:20
  110.0 3.3 %fusion.38 = (f32[128]{0:T(128)S(1)}, bf16[128,2048]{1,0:T(8,128)(2,1)S(1)}) fusion(bf16[128,2048]{1,0:T(8,128)(2,1)} %collective-permute-done.5, bf16[1024,2048]{1,0:T(8,128)(2,1)} %param.38, bf16[256,1024]{0,1:T(8,128)(2,1)} %copy-done.9, s32[]{:T(128)S(6)} %select_n.214, bf16[128,2048]{1,0:T(8,128)(2,1)S(1)} %copy-done.12), kind=kOutput, calls=%fused_computation.49 | convolution fusion | flops 538967936 | bytes 6029828 | tf_op jit(solution)/shard_map/dot_general | solution.py:157
  113.3 1.8 convolution_convert_fusion.3
  115.1 7.1 %all-to-all-start = ((bf16[16,24,2048]{2,1,0:T(8,128)(2,1)}), bf16[16,24,2048]{2,1,0:T(8,128)(2,1)}, u32[]{:S(2)}, u32[]{:S(2)}) async-start(bf16[16,24,2048]{2,1,0:T(8,128)(2,1)} %bitcast.158), calls=%async_computation | async-start | bytes 3145728 | tf_op jit(solution)/shard_map/all_to_all | solution.py:201
  122.4 3.0 %collective-permute-start.6 = (bf16[128,2048]{1,0:T(8,128)(2,1)S(1)}, bf16[128,2048]{1,0:T(8,128)(2,1)}, u32[]{:S(2)}, u32[]{:S(2)}) collective-permute-start(bf16[128,2048]{1,0:T(8,128)(2,1)S(1)} %fusion.40), channel_id=1, source_target_pairs={{0,16},{2,18},{4,20},{6,22},{8,24},{10,26},{12,28},{14,30},{16,0},... | collective-permute-start | bytes 1572872 | tf_op jit(solution)/shard_map/ppermute | solution.py:20
  125.4 26.6 %collective-permute-done.6 = bf16[128,2048]{1,0:T(8,128)(2,1)} collective-permute-done((bf16[128,2048]{1,0:T(8,128)(2,1)S(1)}, bf16[128,2048]{1,0:T(8,128)(2,1)}, u32[]{:S(2)}, u32[]{:S(2)}) %collective-permute-start.6) | collective-permute-done | bytes 524320 | tf_op jit(solution)/shard_map/ppermute | solution.py:20
  152.0 3.6 %all-to-all-done = bf16[16,24,2048]{2,1,0:T(8,128)(2,1)} async-done(((bf16[16,24,2048]{2,1,0:T(8,128)(2,1)}), bf16[16,24,2048]{2,1,0:T(8,128)(2,1)}, u32[]{:S(2)}, u32[]{:S(2)}) %all-to-all-start) | async-done | bytes 1572896 | tf_op jit(solution)/shard_map/all_to_all | solution.py:201
  155.6 1.6 convolution_convert_fusion.1
  157.2 26.4 %all_to_all.20 = bf16[16,24,2048]{2,1,0:T(8,128)(2,1)S(1)} all-to-all(bf16[16,24,2048]{2,1,0:T(8,128)(2,1)S(1)} %bitcast.159), channel_id=1, replica_groups={{0,1,2,3,4,5,6,7,8,9,10,11,12,13,14,15},{16,17,18,19,20,21,22,23,24,25,..., dimensions={0} | all-to-all | bytes 3145728 | tf_op jit(solution)/shard_map/all_to_all | solution.py:201
  184.8 1.9 fusion.10
  186.7 5.3 %convolution_convert_fusion = bf16[384,2048]{1,0:T(8,128)(2,1)} fusion(bf16[1,512,2048]{2,1,0:T(8,128)(2,1)S(1)} %copy-done, bf16[384,2048]{1,0:T(8,128)(2,1)} %bitcast.168, bf16[1,2048,512]{2,1,0:T(8,128)(2,1)} %param.43, f32[384,512]{1,0:T(8,128)} %fusion.10), kind=kOutput, calls=%fused_computation | convolution fusion | flops 1612578816 | bytes 8126464 | tf_op jit(solution)/shard_map/dot_general | solution.py:225
  191.9 4.4 %all-to-all-start.2 = ((bf16[16,24,2048]{2,1,0:T(8,128)(2,1)}), bf16[16,24,2048]{2,1,0:T(8,128)(2,1)}, u32[]{:S(2)}, u32[]{:S(2)}) async-start(bf16[16,24,2048]{2,1,0:T(8,128)(2,1)} %bitcast.166), calls=%async_computation.2 | async-start | bytes 3145728 | tf_op jit(solution)/shard_map/all_to_all | solution.py:201
  196.3 4.0 %fusion.12 = f32[384,512]{1,0:T(8,128)} fusion(bf16[384,2048]{1,0:T(8,128)(2,1)} %bitcast.36, bf16[1,2048,512]{2,1,0:T(8,128)(2,1)} %param.42), kind=kOutput, calls=%fused_computation.22 | convolution fusion | flops 805306368 | bytes 4456448 | tf_op jit(solution)/shard_map/dot_general | solution.py:221
  200.3 5.3 %convolution_convert_fusion.2 = bf16[384,2048]{1,0:T(8,128)(2,1)} fusion(bf16[1,512,2048]{2,1,0:T(8,128)(2,1)S(1)} %copy-done, bf16[384,2048]{1,0:T(8,128)(2,1)} %bitcast.36, bf16[1,2048,512]{2,1,0:T(8,128)(2,1)} %param.43, f32[384,512]{1,0:T(8,128)} %fusion.12), kind=kOutput, calls=%fused_computation.2 | convolution fusion | flops 1612578816 | bytes 8126464 | tf_op jit(solution)/shard_map/dot_general | solution.py:225
  205.6 13.2 %all-to-all-done.2 = bf16[16,24,2048]{2,1,0:T(8,128)(2,1)} async-done(((bf16[16,24,2048]{2,1,0:T(8,128)(2,1)}), bf16[16,24,2048]{2,1,0:T(8,128)(2,1)}, u32[]{:S(2)}, u32[]{:S(2)}) %all-to-all-start.2) | async-done | bytes 1572896 | tf_op jit(solution)/shard_map/all_to_all | solution.py:201
  218.9 1.9 convolution_bitcast_fusion.2
  220.8 2.7 fusion.3
  223.4 4.4 %all-to-all-start.3 = ((bf16[16,24,2048]{2,1,0:T(8,128)(2,1)}), bf16[16,24,2048]{2,1,0:T(8,128)(2,1)}, u32[]{:S(2)}, u32[]{:S(2)}) async-start(bf16[16,24,2048]{2,1,0:T(8,128)(2,1)} %bitcast.165), calls=%async_computation.3 | async-start | bytes 3145728 | tf_op jit(solution)/shard_map/all_to_all | solution.py:201
  229.2 2.1 fusion.149
  231.2 29.7 %all-to-all-done.3 = bf16[16,24,2048]{2,1,0:T(8,128)(2,1)} async-done(((bf16[16,24,2048]{2,1,0:T(8,128)(2,1)}), bf16[16,24,2048]{2,1,0:T(8,128)(2,1)}, u32[]{:S(2)}, u32[]{:S(2)}) %all-to-all-start.3) | async-done | bytes 1572896 | tf_op jit(solution)/shard_map/all_to_all | solution.py:201
  261.0 1.9 convolution_bitcast_fusion
  262.8 2.9 %fusion.2 = f32[128,2048]{1,0:T(8,128)} fusion(f32[128,2048]{1,0:T(8,128)S(1)} %convolution_bitcast_fusion, bf16[16,24,2048]{2,1,0:T(8,128)(2,1)} %all-to-all-done.3, f32[128,16]{0,1:T(8,128)S(1)} %get-tuple-element.46, s32[128,16]{0,1:T(8,128)S(1)} %get-tuple-element.44), kind=kOutput, calls=%fused_computation.11 | convolution fusion | flops 201785344 | bytes 3686400 | tf_op jit(solution)/shard_map/dot_general | solution.py:235
  265.7 4.4 %fusion.15 = bf16[128,2048]{1,0:T(8,128)(2,1)} fusion(f32[128,2048]{1,0:T(8,128)} %fusion.2, bf16[512,2048]{1,0:T(8,128)(2,1)} %param.47, bf16[128,2048]{1,0:T(8,128)(2,1)S(1)} %get-tuple-element.75, bf16[2048,512]{1,0:T(8,128)(2,1)} %param.46, bf16[128,2048]{1,0:T(8,128)(2,1)} %collective-permute-done.8, f32[128,512]{1,0:T(8,128)S(1)} %fusion.149, ...), kind=kOutput, calls=%fused_computation.28 | convolution fusion | flops 539885568 | bytes 7086592 | tf_op jit(solution)/shard_map/dot_general | solution.py:178
  (167 shorter events, 54.8 us)
Async XLA Ops:
  0.0 186.7 %copy-start = (bf16[1,512,2048]{2,1,0:T(8,128)(2,1)S(1)}, bf16[1,512,2048]{2,1,0:T(8,128)(2,1)}, u32[]{:S(2)}) copy-start(bf16[1,512,2048]{2,1,0:T(8,128)(2,1)} %param.44) | copy-start | bytes 6291460
  0.0 14.0 %copy-start.25 = (bf16[4,256]{1,0:T(4,128)(2,1)S(1)}, bf16[4,256]{1,0:T(4,128)(2,1)}, u32[]{:S(2)}) copy-start(bf16[4,256]{1,0:T(4,128)(2,1)} %param.33) | copy-start | bytes 6148
  0.0 14.7 %copy-start.19 = (s32[128,4]{0,1:T(4,128)S(1)}, s32[128,4]{0,1:T(4,128)}, u32[]{:S(2)}) copy-start(s32[128,4]{0,1:T(4,128)} %param.40) | copy-start | bytes 6148
  3.2 14.0 %collective-permute-start = (bf16[3,1536]{0,1:T(8,128)(2,1)}, bf16[3,1536]{0,1:T(8,128)(2,1)}, u32[]{:S(2)}, u32[]{:S(2)}) collective-permute-start(bf16[3,1536]{0,1:T(8,128)(2,1)} %copy.131), channel_id=1, source_target_pairs={{0,2},{2,4},{4,6},{6,8},{8,10},{10,12},{12,14},{14,16},{16,18},{18... | collective-permute-start | bytes 27656 | tf_op jit(solution)/shard_map/ppermute | solution.py:14
  10.6 7.9 %copy-start.21 = (pred[128]{0:T(512)(128)(4,1)}, pred[128]{0:T(512)(128)(4,1)S(1)}, u32[]{:S(2)}) copy-start(pred[128]{0:T(512)(128)(4,1)S(1)} %get-tuple-element.76) | copy-start | bytes 388
  10.7 7.9 %copy-start.23 = (pred[128]{0:T(512)(128)(4,1)}, pred[128]{0:T(512)(128)(4,1)S(1)}, u32[]{:S(2)}) copy-start(pred[128]{0:T(512)(128)(4,1)S(1)} %get-tuple-element.77) | copy-start | bytes 388
  13.0 5.7 %copy-start.30 = (f32[1,2,8]{2,1,0:T(2,128)}, f32[1,2,8]{2,1,0:T(2,128)S(1)}, u32[]{:S(2)}) copy-start(f32[1,2,8]{2,1,0:T(2,128)S(1)} %get-tuple-element.59) | copy-start | bytes 196
  14.0 4.6 %copy-start.33 = (f32[16]{0:T(128)}, f32[16]{0:T(128)S(1)}, u32[]{:S(2)}) copy-start(f32[16]{0:T(128)S(1)} %exp.109) | copy-start | bytes 196
  27.0 5.7 %copy-start.31 = (pred[128,32]{0,1:T(8,128)(4,1)S(1)}, pred[128,32]{0,1:T(8,128)(4,1)}, u32[]{:S(2)}) copy-start(pred[128,32]{0,1:T(8,128)(4,1)} %fusion.121) | copy-start | bytes 12292
  29.1 0.8 copy-start.4
  30.7 9.2 %collective-permute-start.1 = (bf16[1040,128]{1,0:T(8,128)(2,1)}, bf16[1040,128]{1,0:T(8,128)(2,1)}, u32[]{:S(2)}, u32[]{:S(2)}) collective-permute-start(bf16[1040,128]{1,0:T(8,128)(2,1)} %pad_maximum_fusion), channel_id=1, source_target_pairs={{0,2},{2,0},{4,6},{6,4},{8,10},{10,8},{12,14},{14,12},{16,18},{18,... | collective-permute-start | bytes 798728 | tf_op jit(solution)/shard_map/ppermute | solution.py:20
  40.9 0.8 copy-start.8
  48.3 9.3 %copy-start.20 = (s32[128,4]{0,1:T(4,128)S(1)}, s32[128,4]{0,1:T(4,128)}, u32[]{:S(2)}) copy-start(s32[128,4]{0,1:T(4,128)} %param.40) | copy-start | bytes 6148
  49.1 11.5 %collective-permute-start.2 = (bf16[1040,128]{1,0:T(8,128)(2,1)}, bf16[1040,128]{1,0:T(8,128)(2,1)}, u32[]{:S(2)}, u32[]{:S(2)}) collective-permute-start(bf16[1040,128]{1,0:T(8,128)(2,1)} %pad_maximum_fusion.1), channel_id=1, source_target_pairs={{0,4},{2,6},{4,0},{6,2},{8,12},{10,14},{12,8},{14,10},{16,20},{18,... | collective-permute-start | bytes 798728 | tf_op jit(solution)/shard_map/ppermute | solution.py:20
  51.9 7.0 %copy-start.14 = (bf16[3,256]{0,1:T(8,128)(2,1)S(1)}, bf16[3,256]{0,1:T(8,128)(2,1)}, u32[]{:S(2)}) copy-start(bf16[3,256]{0,1:T(8,128)(2,1)} %get-tuple-element.38) | copy-start | bytes 4612
  61.6 0.8 copy-start.2
  63.2 0.6 copy-start.27
  74.1 7.0 %collective-permute-start.3 = (bf16[1040,128]{1,0:T(8,128)(2,1)}, bf16[1040,128]{1,0:T(8,128)(2,1)}, u32[]{:S(2)}, u32[]{:S(2)}) collective-permute-start(bf16[1040,128]{1,0:T(8,128)(2,1)} %pad_maximum_fusion.2), channel_id=1, source_target_pairs={{0,8},{2,10},{4,12},{6,14},{8,0},{10,2},{12,4},{14,6},{16,24},{18,... | collective-permute-start | bytes 798728 | tf_op jit(solution)/shard_map/ppermute | solution.py:20
  77.2 9.6 %copy-start.22 = (pred[128]{0:T(512)(128)(4,1)S(1)}, pred[128]{0:T(512)(128)(4,1)}, u32[]{:S(2)}) copy-start(pred[128]{0:T(512)(128)(4,1)} %copy-done.21) | copy-start | bytes 388
  77.2 9.6 %copy-start.24 = (pred[128]{0:T(512)(128)(4,1)S(1)}, pred[128]{0:T(512)(128)(4,1)}, u32[]{:S(2)}) copy-start(pred[128]{0:T(512)(128)(4,1)} %copy-done.23) | copy-start | bytes 388
  82.2 0.8 copy-start.7
  84.6 7.6 %copy-start.13 = (f32[2,2,128,128]{3,2,1,0:T(8,128)S(1)}, f32[2,2,128,128]{3,2,1,0:T(8,128)}, u32[]{:S(2)}) copy-start(f32[2,2,128,128]{3,2,1,0:T(8,128)} %fusion.103) | copy-start | bytes 786436
  87.0 9.7 %copy-start.35 = (f32[16]{0:T(128)S(1)}, f32[16]{0:T(128)}, u32[]{:S(2)}) copy-start(f32[16]{0:T(128)} %get-tuple-element.14) | copy-start | bytes 196
  87.0 9.8 %copy-start.34 = (f32[16]{0:T(128)S(1)}, f32[16]{0:T(128)}, u32[]{:S(2)}) copy-start(f32[16]{0:T(128)} %get-tuple-element.20) | copy-start | bytes 196
  87.0 11.6 %collective-permute-start.4 = (bf16[1040,128]{1,0:T(8,128)(2,1)S(1)}, bf16[1040,128]{1,0:T(8,128)(2,1)}, u32[]{:S(2)}, u32[]{:S(2)}) collective-permute-start(bf16[1040,128]{1,0:T(8,128)(2,1)S(1)} %pad_maximum_fusion.3), channel_id=1, source_target_pairs={{0,16},{2,18},{4,20},{6,22},{8,24},{10,26},{12,28},{14,30},{1,17},... | collective-permute-start | bytes 798728 | tf_op jit(solution)/shard_map/ppermute | solution.py:20
  97.5 3.7 %copy-start.6 = (f32[2,2,8,64,128]{4,3,2,1,0:T(8,128)S(1)}, f32[2,2,8,64,128]{4,3,2,1,0:T(8,128)}, u32[]{:S(2)}) copy-start(f32[2,2,8,64,128]{4,3,2,1,0:T(8,128)} %get-tuple-element.71) | copy-start | bytes 3145732
  97.5 3.7 %copy-start.32 = (f32[2,8]{1,0:T(2,128)S(1)}, f32[2,8]{1,0:T(2,128)}, u32[]{:S(2)}) copy-start(f32[2,8]{1,0:T(2,128)} %fusion.134) | copy-start | bytes 196
  99.6 1.8 copy-start.5
  99.6 1.8 copy-start.11
  99.6 1.8 copy-start.16
  99.6 1.8 copy-start.29
  101.5 1.4 copy-start.3
  102.0 0.9 copy-start.28
  102.0 2.2 copy-start.1
  104.2 0.8 copy-start.9
  104.2 0.9 copy-start.17
  104.2 0.9 copy-start.18
  104.2 5.8 %copy-start.12 = (bf16[128,2048]{1,0:T(8,128)(2,1)S(1)}, bf16[128,2048]{1,0:T(8,128)(2,1)}, u32[]{:S(2)}) copy-start(bf16[128,2048]{1,0:T(8,128)(2,1)} %param.24) | copy-start | bytes 1572868
  105.0 5.0 %collective-permute-start.5 = (bf16[128,2048]{1,0:T(8,128)(2,1)S(1)}, bf16[128,2048]{1,0:T(8,128)(2,1)}, u32[]{:S(2)}, u32[]{:S(2)}) collective-permute-start(bf16[128,2048]{1,0:T(8,128)(2,1)S(1)} %convolution_convert_fusion.4), channel_id=1, source_target_pairs={{0,1},{1,0},{2,3},{3,2},{4,5},{5,4},{6,7},{7,6},{8,9},{9,8},{10,11... | collective-permute-start | bytes 1572872 | tf_op jit(solution)/shard_map/ppermute | solution.py:163
  105.1 4.7 %collective-permute-start.7 = (f32[2,128,16]{1,2,0:T(8,128)S(1)}, f32[2,128,16]{1,2,0:T(8,128)S(1)}, u32[]{:S(2)}, u32[]{:S(2)}) collective-permute-start(f32[2,128,16]{1,2,0:T(8,128)S(1)} %get-tuple-element.42), channel_id=1, source_target_pairs={{0,16},{2,18},{4,20},{6,22},{8,24},{10,26},{12,28},{14,30},{16,0},... | collective-permute-start | bytes 49160 | tf_op jit(solution)/shard_map/ppermute | solution.py:20
  110.0 3.3 %copy-start.15 = (f32[2048]{0:T(1024)S(1)}, f32[2048]{0:T(1024)}, u32[]{:S(2)}) copy-start(f32[2048]{0:T(1024)} %param.39) | copy-start | bytes 24580
  115.1 40.5 %all-to-all-start = ((bf16[16,24,2048]{2,1,0:T(8,128)(2,1)}), bf16[16,24,2048]{2,1,0:T(8,128)(2,1)}, u32[]{:S(2)}, u32[]{:S(2)}) async-start(bf16[16,24,2048]{2,1,0:T(8,128)(2,1)} %bitcast.158), calls=%async_computation | async-start | bytes 3145728 | tf_op jit(solution)/shard_map/all_to_all | solution.py:201
  122.4 29.6 %collective-permute-start.6 = (bf16[128,2048]{1,0:T(8,128)(2,1)S(1)}, bf16[128,2048]{1,0:T(8,128)(2,1)}, u32[]{:S(2)}, u32[]{:S(2)}) collective-permute-start(bf16[128,2048]{1,0:T(8,128)(2,1)S(1)} %fusion.40), channel_id=1, source_target_pairs={{0,16},{2,18},{4,20},{6,22},{8,24},{10,26},{12,28},{14,30},{16,0},... | collective-permute-start | bytes 1572872 | tf_op jit(solution)/shard_map/ppermute | solution.py:20
  157.2 27.6 %copy-start.36 = (bf16[1,2048,512]{2,1,0:T(8,128)(2,1)S(1)}, bf16[1,2048,512]{2,1,0:T(8,128)(2,1)}, u32[]{:S(2)}) copy-start(bf16[1,2048,512]{2,1,0:T(8,128)(2,1)} %param.42) | copy-start | bytes 6291460
  183.6 1.2 copy-start.10
  191.9 26.9 %all-to-all-start.2 = ((bf16[16,24,2048]{2,1,0:T(8,128)(2,1)}), bf16[16,24,2048]{2,1,0:T(8,128)(2,1)}, u32[]{:S(2)}, u32[]{:S(2)}) async-start(bf16[16,24,2048]{2,1,0:T(8,128)(2,1)} %bitcast.166), calls=%async_computation.2 | async-start | bytes 3145728 | tf_op jit(solution)/shard_map/all_to_all | solution.py:201
  223.4 37.5 %all-to-all-start.3 = ((bf16[16,24,2048]{2,1,0:T(8,128)(2,1)}), bf16[16,24,2048]{2,1,0:T(8,128)(2,1)}, u32[]{:S(2)}, u32[]{:S(2)}) async-start(bf16[16,24,2048]{2,1,0:T(8,128)(2,1)} %bitcast.165), calls=%async_computation.3 | async-start | bytes 3145728 | tf_op jit(solution)/shard_map/all_to_all | solution.py:201
  227.8 37.9 %collective-permute-start.8 = (bf16[128,2048]{1,0:T(8,128)(2,1)}, bf16[128,2048]{1,0:T(8,128)(2,1)}, u32[]{:S(2)}, u32[]{:S(2)}) collective-permute-start(bf16[128,2048]{1,0:T(8,128)(2,1)} %fusion.3), channel_id=1, source_target_pairs={{0,16},{2,18},{4,20},{6,22},{8,24},{10,26},{12,28},{14,30},{16,0},... | collective-permute-start | bytes 1572872 | tf_op jit(solution)/shard_map/ppermute | solution.py:20
  (1 other events, 0.5 us)
